TPU v7x, 32 devices: a whole 2x2x4 slice. The times are simulated.
32 devices in a mesh: rep: 2 (over x), fs: 8 (over z, y), tp: 2 (over core).
Axes of the slice: x: 2, y: 2, z: 4, core: 2. Of those that a mesh axis runs over, the one named last changes fastest.
Arguments:
- tokens: bfloat16 [16, 192, 2048], P(('rep', 'fs'), 'tp'), may hold values from -6 to 6
- mix_gain: float32 [2048], replicated, may hold values from 0.1 to 1.9
- w_query: float32 [2048, 2048], P('fs', 'tp'), may hold values from -0.125 to 0.125
- w_key: float32 [2048, 2048], P('fs', 'tp'), may hold values from -0.125 to 0.125
- w_value: float32 [2048, 2048], P('fs', 'tp'), may hold values from -0.125 to 0.125
- w_out: float32 [2048, 2048], P('tp', 'fs'), may hold values from -0.125 to 0.125
- scale_query: float32 [2048], P('tp'), may hold values from 0.1 to 1.9
- scale_key: float32 [2048], P('tp'), may hold values from 0.1 to 1.9
- scale_value: float32 [2048], P('tp'), may hold values from 0.1 to 1.9
- scale_out: float32 [2048], replicated, may hold values from 0.1 to 1.9
- decay_rate: float32 [8], P('tp'), may hold values from 0.003 to 0.08
- mlp_gain: float32 [2048], replicated, may hold values from 0.1 to 1.9
- w_gate: float32 [2048, 3072], P('fs', 'tp'), may hold values from -0.125 to 0.125
- w_up: float32 [2048, 3072], P('fs', 'tp'), may hold values from -0.125 to 0.125
- w_down: float32 [3072, 2048], P('tp', 'fs'), may hold values from -0.109375 to 0.109375
- scale_gate: float32 [3072], P('tp'), may hold values from 0.1 to 1.9
- scale_up: float32 [3072], P('tp'), may hold values from 0.1 to 1.9
- scale_down: float32 [2048], replicated, may hold values from 0.1 to 1.9
Outputs:
- layer_out: bfloat16 [16, 192, 2048], P(('rep', 'fs'), 'tp')
All inputs are finite; a program needn't handle non-finite values.
Results may differ from a plain program's by a relative error of at most 0.015.
Values may be sent and summed in bfloat16 or wider, within the bound.
A program may use at most 64 MiB of HBM per device.

v0:
```python
import jax
import jax.numpy as jnp
from jax import lax
from jax.sharding import PartitionSpec as P

HEAD_DIM = 256
BLOCK = 64
EPS = 1e-06
ROPE_BASE = 10000.0


def rms_scale(values, gain):
    values = values.astype(jnp.float32)
    return values * lax.rsqrt(jnp.mean(values * values, axis=-1, keepdims=True) + EPS) * gain


def rotary(values, positions):
    width = values.shape[-1]
    half = width // 2
    inv_freq = 1.0 / ROPE_BASE ** (jnp.arange(0, width, 2, dtype=jnp.float32) / width)
    angles = positions.astype(jnp.float32)[:, None] * inv_freq[None, :]
    cosine = jnp.cos(angles)[:, None, :]
    sine = jnp.sin(angles)[:, None, :]
    first = values[..., :half]
    second = values[..., half:]
    return jnp.concatenate(
        [first * cosine - second * sine, first * sine + second * cosine], axis=-1
    )


def retention(query, keyed, valued, rates):
    length, heads, width = query.shape
    nblocks = length // BLOCK

    def split(values):
        return values.reshape(nblocks, BLOCK, heads, width).transpose(0, 2, 1, 3)

    log_gamma = -rates
    inside = jnp.arange(BLOCK, dtype=jnp.float32)
    distance = inside[:, None] - inside[None, :]
    inner_product = jnp.where(
        distance[None] >= 0.0,
        jnp.exp(log_gamma[:, None, None] * jnp.maximum(distance, 0.0)[None]),
        0.0,
    )
    query_decay = jnp.exp(log_gamma[:, None] * (inside[None, :] + 1.0))
    key_decay_factor = jnp.exp(log_gamma[:, None] * (BLOCK - 1.0 - inside[None, :]))
    block_decay = jnp.exp(log_gamma * BLOCK)

    def advance(state, blocks):
        query_block_tile, key_block_tile, value_block_tile = blocks
        attention_scores = jnp.einsum(
            "frk,fvk->frv", query_block_tile, key_block_tile, preferred_element_type=jnp.float32
        )
        decay_weights = (attention_scores * inner_product).astype(jnp.bfloat16)
        local = jnp.einsum(
            "hnm,hmv->hnv", decay_weights, value_block_tile, preferred_element_type=jnp.float32
        )
        carried = jnp.einsum(
            "hnd,hdv->hnv",
            query_block_tile.astype(jnp.float32) * query_decay[:, :, None],
            state,
            precision=lax.Precision.HIGHEST,
        )
        state_update = jnp.einsum(
            "asf,asp->afp",
            key_block_tile.astype(jnp.float32) * key_decay_factor[:, :, None],
            value_block_tile.astype(jnp.float32),
            precision=lax.Precision.HIGHEST,
        )
        return (state * block_decay[:, None, None] + state_update, local + carried)

    initial = jnp.zeros((heads, width, width), jnp.float32)
    _, outs = lax.scan(advance, initial, (split(query), split(keyed), split(valued)))
    return outs.transpose(0, 2, 1, 3).reshape(length, heads, width)


def per_device(
    tokens,
    mix_gain,
    w_query,
    w_key,
    w_value,
    w_out,
    scale_query,
    scale_key,
    scale_value,
    scale_out,
    decay_rate,
    mlp_gain,
    w_gate,
    w_up,
    w_down,
    scale_gate,
    scale_up,
    scale_down,
):
    own_rows = tokens[0]
    all_rows = lax.all_gather(own_rows, "tp", axis=0, tiled=True)
    gathered = rms_scale(all_rows, mix_gain).astype(jnp.bfloat16)
    length = gathered.shape[0]
    width = w_query.shape[1]
    shards = (
        lax.all_gather(w_query.astype(jnp.bfloat16), "fs", axis=0, tiled=True),
        lax.all_gather(w_key.astype(jnp.bfloat16), "fs", axis=0, tiled=True),
        lax.all_gather(w_value.astype(jnp.bfloat16), "fs", axis=0, tiled=True),
    )
    columns = gathered
    query_raw, key_raw, value_raw = tuple(
        (jnp.dot(columns, shard, preferred_element_type=jnp.float32) for shard in shards)
    )
    positions = jnp.arange(length)
    heads_here = width // HEAD_DIM
    query_rows = rotary(
        (query_raw * scale_query).reshape(length, heads_here, HEAD_DIM), positions
    ).astype(jnp.bfloat16)
    key_rows = rotary(
        (key_raw * scale_key).reshape(length, heads_here, HEAD_DIM), positions
    ).astype(jnp.bfloat16)
    value_rows = (
        (value_raw * scale_value).reshape(length, heads_here, HEAD_DIM).astype(jnp.bfloat16)
    )
    retained = retention(query_rows, key_rows, value_rows, decay_rate)
    attended = rms_scale(retained, 1.0).astype(jnp.bfloat16).reshape(length, width)
    out_whole = lax.all_gather(w_out.astype(jnp.bfloat16), "fs", axis=1, tiled=True)
    picked = attended
    mixed = lax.psum_scatter(
        (jnp.dot(picked, out_whole, preferred_element_type=jnp.float32) * scale_out).astype(
            jnp.bfloat16
        ),
        "tp",
        scatter_dimension=0,
        tiled=True,
    ).astype(jnp.float32)
    hidden_state = (own_rows.astype(jnp.float32) + mixed).astype(jnp.bfloat16)
    mlp_in = rms_scale(hidden_state, mlp_gain).astype(jnp.bfloat16)
    mlp_rows_in = lax.all_gather(mlp_in, "tp", axis=0, tiled=True)
    shards = (
        lax.all_gather(w_gate.astype(jnp.bfloat16), "fs", axis=0, tiled=True),
        lax.all_gather(w_up.astype(jnp.bfloat16), "fs", axis=0, tiled=True),
    )
    columns = mlp_rows_in
    gate_val, up_val = tuple(
        (jnp.dot(columns, shard, preferred_element_type=jnp.float32) for shard in shards)
    )
    down_whole = lax.all_gather(w_down.astype(jnp.bfloat16), "fs", axis=1, tiled=True)
    inner_product = (jax.nn.silu(gate_val * scale_gate) * (up_val * scale_up)).astype(jnp.bfloat16)
    picked = inner_product
    channel = lax.psum_scatter(
        (jnp.dot(picked, down_whole, preferred_element_type=jnp.float32) * scale_down).astype(
            jnp.bfloat16
        ),
        "tp",
        scatter_dimension=0,
        tiled=True,
    ).astype(jnp.float32)
    return (hidden_state.astype(jnp.float32) + channel).astype(jnp.bfloat16)[None]


def solution(mesh):
    in_specs = (
        P(("rep", "fs"), "tp", None),
        P(),
        P("fs", "tp"),
        P("fs", "tp"),
        P("fs", "tp"),
        P("tp", "fs"),
        P("tp"),
        P("tp"),
        P("tp"),
        P(),
        P("tp"),
        P(),
        P("fs", "tp"),
        P("fs", "tp"),
        P("tp", "fs"),
        P("tp"),
        P("tp"),
        P(),
    )
    out_specs = P(("rep", "fs"), "tp", None)
    return jax.shard_map(
        per_device, mesh=mesh, in_specs=in_specs, out_specs=out_specs, check_vma=False
    )
```

profile of v0, /device:TPU:0, one launch (start us, length us, event | category | flops | bytes accessed | tf_op | source)
XLA Modules:
  0.0 641.8 jit_solution(169841490198912978)
XLA Ops:
  6.5 2.2 convert_element_type.108
  8.8 0.0 all-gather.13.cloned.1.call-start
  8.8 0.9 convert_element_type.113
  9.7 0.0 all-gather.11.cloned.1.call-start
  9.8 0.4 copy-done.7
  10.1 0.9 convert_element_type.110
  11.1 0.0 all-gather.15.cloned.1.call-start
  11.1 0.8 convert_element_type.115
  12.0 0.0 reduce-scatter.3.cloned.1.call-start
  12.2 2.5 all-gather
  14.7 0.2 fusion.52
  14.9 0.4 multiply_cosine_fusion
  15.3 69.7 %all-gather.9.cloned.1.call-done = bf16[2048,1024]{1,0:T(8,128)(2,1)} async-done(((bf16[256,1024]{1,0:T(8,128)(2,1)}), bf16[2048,1024]{1,0:T(8,128)(2,1)}) %all-gather.9.cloned.1.call-update) | async-done | bytes 4194320 | tf_op jit(solution)/shard_map/all_gather | solution.py:105
  85.0 4.1 convolution_multiply_fusion.7
  89.2 1.5 reshape.164
  90.7 67.8 %all-gather.13.cloned.1.call-done = bf16[2048,1024]{1,0:T(8,128)(2,1)} async-done(((bf16[256,1024]{1,0:T(8,128)(2,1)}), bf16[2048,1024]{1,0:T(8,128)(2,1)}) %all-gather.13.cloned.1.call-update) | async-done | bytes 4194320 | tf_op jit(solution)/shard_map/all_gather | solution.py:104
  158.5 4.1 convolution_multiply_fusion.5
  162.6 2.4 reshape.165
  165.1 66.9 %all-gather.11.cloned.1.call-done = bf16[2048,1024]{1,0:T(8,128)(2,1)} async-done(((bf16[256,1024]{1,0:T(8,128)(2,1)}), bf16[2048,1024]{1,0:T(8,128)(2,1)}) %all-gather.11.cloned.1.call-update) | async-done | bytes 4194320 | tf_op jit(solution)/shard_map/all_gather | solution.py:106
  232.0 4.0 fusion.55
  236.0 1.3 convert_element_type.112
  237.3 1.3 fusion.70
  238.6 0.2 subtract_convert_fusion
  238.8 0.1 maximum_bitcast_fusion.1
  238.9 0.1 maximum_bitcast_fusion
  238.9 8.3 %while.15 = (s32[]{:T(128)}, f32[4,256,256]{2,1,0:T(8,128)S(1)}, f32[3,4,64,256]{3,2,1,0:T(8,128)}, f32[4]{0:T(128)S(1)}, bf16[3,4,64,256]{3,2,0,1:T(8,128)(2,1)...) while((s32[]{:T(128)}, f32[4,256,256]{2,1,0:T(8,128)S(1)}, ...), condition=%wide.region_2.3_spmd.clone.clone.clone, body=%wide.region_1.2_spmd.clone.clone.clone.sunk | while | flops 420872704 | bytes 4770468 | solution.py:74
  238.9 0.1 multiply_exponential_fusion.4
  239.0 0.8 fusion.98
  239.8 1.0 fusion.99
  240.8 0.8 convolution_add_fusion.3
  241.7 0.1 multiply_exponential_fusion.4
  241.8 0.8 fusion.98
  242.6 1.0 fusion.99
  243.6 0.8 convolution_add_fusion.3
  244.5 0.1 multiply_exponential_fusion.4
  244.5 0.8 fusion.98
  245.4 1.0 fusion.99
  246.4 0.8 convolution_add_fusion.3
  247.2 1.4 multiply_reduce_fusion
  248.6 0.1 copy.46
  248.8 0.3 mul.353
  249.0 0.1 copy.55
  249.2 0.5 copy.43
  249.7 0.1 copy.54
  249.9 57.2 %all-gather.15.cloned.1.call-done = bf16[1024,2048]{1,0:T(8,128)(2,1)} async-done(((bf16[1024,256]{1,0:T(8,128)(2,1)}), bf16[1024,2048]{1,0:T(8,128)(2,1)}) %all-gather.15.cloned.1.call-update) | async-done | bytes 4194320 | tf_op jit(solution)/shard_map/all_gather | solution.py:125
  307.1 4.2 fusion.49
  311.3 0.0 all-gather.17.cloned.1.call-start
  311.4 1.0 convert_element_type.121
  312.4 0.0 all-gather.19.cloned.1.call-start
  312.4 0.6 copy-done.4
  313.0 1.0 convert_element_type.122
  314.0 0.0 all-gather.21.cloned.1.call-start
  314.1 1.0 convert_element_type.124
  315.2 2.6 reduce-scatter.3.cloned.1.call-done
  317.8 1.2 fusion.56
  319.0 1.2 fusion.58
  320.2 2.5 all_gather.32
  322.8 96.9 %all-gather.17.cloned.1.call-done = bf16[2048,1536]{1,0:T(8,128)(2,1)} async-done(((bf16[256,1536]{1,0:T(8,128)(2,1)}), bf16[2048,1536]{1,0:T(8,128)(2,1)}) %all-gather.17.cloned.1.call-update) | async-done | bytes 6291472 | tf_op jit(solution)/shard_map/all_gather | solution.py:139
  419.7 4.2 convolution_multiply_fusion.2
  423.9 94.9 %all-gather.19.cloned.1.call-done = bf16[2048,1536]{1,0:T(8,128)(2,1)} async-done(((bf16[256,1536]{1,0:T(8,128)(2,1)}), bf16[2048,1536]{1,0:T(8,128)(2,1)}) %all-gather.19.cloned.1.call-update) | async-done | bytes 6291472 | tf_op jit(solution)/shard_map/all_gather | solution.py:140
  518.8 99.7 %all-gather.21.cloned.1.call-done = bf16[1536,2048]{1,0:T(8,128)(2,1)} async-done(((bf16[1536,256]{1,0:T(8,128)(2,1)}), bf16[1536,2048]{1,0:T(8,128)(2,1)}) %all-gather.21.cloned.1.call-update) | async-done | bytes 6291472 | tf_op jit(solution)/shard_map/all_gather | solution.py:146
  618.6 8.3 %fusion.50 = bf16[192,2048]{1,0:T(8,128)(2,1)} fusion(bf16[1536,2048]{1,0:T(8,128)(2,1)} %all-gather.21.cloned.1.call-done, f32[2048]{0:T(1024)S(1)} %copy-done.13, bf16[192,2048]{1,0:T(8,128)(2,1)S(1)} %all_gather.32, bf16[2048,1536]{1,0:T(8,128)(2,1)} %all-gather.19.cloned.1.call-done, f32[192,1536]{1,0:T(8,128)S(1)} %convolution_multiply_fusion.2, ...), kind=kOutput, calls=%fused_computation.51 | convolution fusion | flops 2418769920 | bytes 15349760 | tf_op jit(solution)/shard_map/dot_general | solution.py:150
  626.9 6.5 %reduce-scatter.5.cloned.1.call-done = bf16[96,2048]{1,0:T(8,128)(2,1)} async-done(((bf16[192,2048]{1,0:T(8,128)(2,1)}), bf16[96,2048]{1,0:T(8,128)(2,1)}) %reduce-scatter.5.cloned.1.call-update) | async-done | bytes 393232 | tf_op jit(solution)/shard_map/reduce_scatter | solution.py:149
  633.4 1.9 fusion.63
  (59 shorter events, 0.4 us)
Async XLA Ops:
  6.5 2.3 copy-start.6
  6.5 78.5 %all-gather.9.cloned.1.call-start = ((), (), s32[]{:S(2)}) async-start(), calls=%async_computation.2 | async-start | bytes 4718592 | tf_op jit(solution)/shard_map/all_gather | solution.py:105
  8.7 1.4 copy-start.7
  8.8 149.7 %all-gather.13.cloned.1.call-start = ((), (), s32[]{:S(2)}) async-start(), calls=%async_computation.4 | async-start | bytes 4718592 | tf_op jit(solution)/shard_map/all_gather | solution.py:104
  9.7 1.4 copy-start.8
  9.7 222.3 %all-gather.11.cloned.1.call-start = ((), (), s32[]{:S(2)}) async-start(), calls=%async_computation.3 | async-start | bytes 4718592 | tf_op jit(solution)/shard_map/all_gather | solution.py:106
  11.0 1.1 copy-start
  11.1 296.0 %all-gather.15.cloned.1.call-start = ((), (), s32[]{:S(2)}) async-start(), calls=%async_computation.5 | async-start | bytes 4718592 | tf_op jit(solution)/shard_map/all_gather | solution.py:125
  12.0 2.9 copy-start.18
  12.0 73.0 %copy-start.11 = (f32[2048]{0:T(1024)S(1)}, f32[2048]{0:T(1024)}, u32[]{:S(2)}) copy-start(f32[2048]{0:T(1024)} %param.21) | copy-start | bytes 24580
  12.0 73.0 %copy-start.15 = (f32[1024]{0:T(1024)S(1)}, f32[1024]{0:T(1024)}, u32[]{:S(2)}) copy-start(f32[1024]{0:T(1024)} %param.27) | copy-start | bytes 12292
  12.0 305.8 %reduce-scatter.3.cloned.1.call-start = ((), (), s32[]{:S(2)}) async-start(), calls=%async_computation.6 | async-start | bytes 1179648 | tf_op jit(solution)/shard_map/reduce_scatter | solution.py:127
  89.2 69.3 %copy-start.16 = (f32[1024]{0:T(1024)S(1)}, f32[1024]{0:T(1024)}, u32[]{:S(2)}) copy-start(f32[1024]{0:T(1024)} %param.26) | copy-start | bytes 12292
  162.6 69.3 %copy-start.17 = (f32[1024]{0:T(1024)S(1)}, f32[1024]{0:T(1024)}, u32[]{:S(2)}) copy-start(f32[1024]{0:T(1024)} %param.28) | copy-start | bytes 12292
  247.2 2.0 copy-start.2
  249.2 57.9 %copy-start.9 = (f32[2048]{0:T(1024)S(1)}, f32[2048]{0:T(1024)}, u32[]{:S(2)}) copy-start(f32[2048]{0:T(1024)} %param.29) | copy-start | bytes 24580
  307.1 4.3 copy-start.3
  311.3 1.7 copy-start.4
  311.3 108.4 %all-gather.17.cloned.1.call-start = ((), (), s32[]{:S(2)}) async-start(), calls=%async_computation.7 | async-start | bytes 7077888 | tf_op jit(solution)/shard_map/all_gather | solution.py:139
  312.4 1.7 copy-start.5
  312.4 206.4 %all-gather.19.cloned.1.call-start = ((), (), s32[]{:S(2)}) async-start(), calls=%async_computation.8 | async-start | bytes 7077888 | tf_op jit(solution)/shard_map/all_gather | solution.py:140
  314.0 5.0 copy-start.10
  314.0 304.5 %all-gather.21.cloned.1.call-start = ((), (), s32[]{:S(2)}) async-start(), calls=%async_computation.9 | async-start | bytes 7077888 | tf_op jit(solution)/shard_map/all_gather | solution.py:146
  315.1 104.6 %copy-start.12 = (f32[1536]{0:T(1024)S(1)}, f32[1536]{0:T(1024)}, u32[]{:S(2)}) copy-start(f32[1536]{0:T(1024)} %param.35) | copy-start | bytes 18436
  315.1 318.2 %reduce-scatter.5.cloned.1.call-start = ((), (), s32[]{:S(2)}) async-start(), calls=%async_computation.10 | async-start | bytes 1179648 | tf_op jit(solution)/shard_map/reduce_scatter | solution.py:149
  322.8 295.8 %copy-start.13 = (f32[2048]{0:T(1024)S(1)}, f32[2048]{0:T(1024)}, u32[]{:S(2)}) copy-start(f32[2048]{0:T(1024)} %param.37) | copy-start | bytes 24580
  322.8 295.8 %copy-start.14 = (f32[1536]{0:T(1024)S(1)}, f32[1536]{0:T(1024)}, u32[]{:S(2)}) copy-start(f32[1536]{0:T(1024)} %param.36) | copy-start | bytes 18436
  423.9 209.5 %copy-start.1 = (bf16[96,2048]{1,0:T(8,128)(2,1)S(1)}, bf16[96,2048]{1,0:T(8,128)(2,1)}, u32[]{:S(2)}) copy-start(bf16[96,2048]{1,0:T(8,128)(2,1)} %reduce-scatter.3.cloned.1.call-done) | copy-start | bytes 1179652
Sparse Core Ops, SparseCore 0:
  9.5 75.5 all-gather.8
  87.1 71.3 all-gather.12
  160.6 71.3 all-gather.10
  233.9 73.1 all-gather.14
  311.4 6.3 reduce-scatter.2
  319.8 99.8 all-gather.16
  421.9 96.9 all-gather.18
  520.9 97.6 all-gather.20
  627.0 6.3 reduce-scatter.4
where the time goes:
time: 642 us
  waiting for transfers between devices  563 us (88%)
  matrix products  36.9 us (6%)
  other arithmetic  14.7 us (2%)
  between operations  13.5 us (2%)
  local copies, waits for them, and re-layouts  8.76 us (1%)
    all_gather x1, waiting for transfers between devices, per_device(): lax.all_gather(w_down.astype(jnp.bfloat16), 'fs', axis=1, tiled=True)  99.7 us
    all_gather x1, waiting for transfers between devices, per_device(): lax.all_gather(w_gate.astype(jnp.bfloat16), 'fs', axis=0, tiled=True)  96.9 us
    all_gather x1, waiting for transfers between devices, per_device(): lax.all_gather(w_up.astype(jnp.bfloat16), 'fs', axis=0, tiled=True)  94.9 us
    all_gather x1, waiting for transfers between devices, per_device(): lax.all_gather(w_key.astype(jnp.bfloat16), 'fs', axis=0, tiled=True)  69.7 us
    all_gather x1, waiting for transfers between devices, per_device(): lax.all_gather(w_query.astype(jnp.bfloat16), 'fs', axis=0, tiled=True)  67.8 us
    all_gather x1, waiting for transfers between devices, per_device(): lax.all_gather(w_value.astype(jnp.bfloat16), 'fs', axis=0, tiled=True)  66.9 us
    all_gather x1, waiting for transfers between devices, per_device(): lax.all_gather(w_out.astype(jnp.bfloat16), 'fs', axis=1, tiled=True)  57.2 us
    dot_general x4, matrix products, per_device(): jnp.dot(columns, shard, preferred_element_type=jnp.float32)  16.4 us
  transfers between devices with their start and end apart: 9, of which 9 were waited for; matrix products, arithmetic and copies ran while one was open for 7% of the time, Pallas kernels for 0%

commit v1 on v0

--- a/solution.py
+++ b/solution.py
@@ -143,7 +143,9 @@
     gate_val, up_val = tuple(
         (jnp.dot(columns, shard, preferred_element_type=jnp.float32) for shard in shards)
     )
-    down_whole = lax.all_gather(w_down.astype(jnp.bfloat16), "fs", axis=1, tiled=True)
+    own = w_down.astype(jnp.bfloat16)
+    shards_2 = lax.all_gather(own, "fs")
+    down_whole = jnp.concatenate(shards_2, axis=1)
     inner_product = (jax.nn.silu(gate_val * scale_gate) * (up_val * scale_up)).astype(jnp.bfloat16)
     picked = inner_product
     channel = lax.psum_scatter(

time: 642 us -> 643 us (level)
  waiting for transfers between devices: 563 us -> 553 us
  local copies, waits for them, and re-layouts: 8.76 us -> 17.5 us
    reshape x0 -> x1, local copies, waits for them, and re-layouts: none -> 8.76 us  [per_device(): down_whole = jnp.concatenate(shards_2, axis=1)]
    all_gather x1, waiting for transfers between devices: 96.9 us -> 90.3 us  [per_device(): lax.all_gather(w_gate.astype(jnp.bfloat16), 'fs', axis=0, tiled=True)]
  transfers between devices with their start and end apart: 9 -> 9, of which waited for: 9 -> 9; matrix products, arithmetic and copies ran while one was open for 7% -> 8% of each run, Pallas kernels for 0% -> 0%
where the time goes in v1:
time: 643 us; the launch traced here: 642 us
  waiting for transfers between devices  553 us (86%)
  matrix products  37.7 us (6%)
  local copies, waits for them, and re-layouts  17.5 us (3%)
  other arithmetic  14.7 us (2%)
  between operations  13.5 us (2%)
    all_gather x1, waiting for transfers between devices, per_device(): shards_2 = lax.all_gather(own, 'fs')  96.9 us
    all_gather x1, waiting for transfers between devices, per_device(): lax.all_gather(w_up.astype(jnp.bfloat16), 'fs', axis=0, tiled=True)  95 us
    all_gather x1, waiting for transfers between devices, per_device(): lax.all_gather(w_gate.astype(jnp.bfloat16), 'fs', axis=0, tiled=True)  90.3 us
    all_gather x1, waiting for transfers between devices, per_device(): lax.all_gather(w_key.astype(jnp.bfloat16), 'fs', axis=0, tiled=True)  69.7 us
    all_gather x1, waiting for transfers between devices, per_device(): lax.all_gather(w_query.astype(jnp.bfloat16), 'fs', axis=0, tiled=True)  67.8 us
    all_gather x1, waiting for transfers between devices, per_device(): lax.all_gather(w_value.astype(jnp.bfloat16), 'fs', axis=0, tiled=True)  66.9 us
    all_gather x1, waiting for transfers between devices, per_device(): lax.all_gather(w_out.astype(jnp.bfloat16), 'fs', axis=1, tiled=True)  57.2 us
    dot_general x4, matrix products, per_device(): jnp.dot(columns, shard, preferred_element_type=jnp.float32)  16.4 us
  transfers between devices with their start and end apart: 9, of which 9 were waited for; matrix products, arithmetic and copies ran while one was open for 8% of the time, Pallas kernels for 0%

profile of v1, /device:TPU:0, one launch (start us, length us, event | category | flops | bytes accessed | tf_op | source)
XLA Modules:
  0.0 641.9 jit_solution(3074652596309704122)
XLA Ops:
  6.5 2.2 convert_element_type.108
  8.8 0.0 all-gather.14.cloned.1.call-start
  8.8 0.9 convert_element_type.113
  9.7 0.0 all-gather.12.cloned.1.call-start
  9.8 0.4 copy-done.7
  10.1 0.9 convert_element_type.110
  11.1 0.8 convert_element_type.115
  12.0 0.0 reduce-scatter.3.cloned.1.call-start
  12.2 2.5 all-gather
  14.7 0.2 fusion.52
  14.9 0.4 multiply_cosine_fusion
  15.3 69.7 %all-gather.10.cloned.1.call-done = bf16[2048,1024]{1,0:T(8,128)(2,1)} async-done(((bf16[256,1024]{1,0:T(8,128)(2,1)}), bf16[2048,1024]{1,0:T(8,128)(2,1)}) %all-gather.10.cloned.1.call-update) | async-done | bytes 4194320 | tf_op jit(solution)/shard_map/all_gather | solution.py:105
  85.0 4.1 convolution_multiply_fusion.7
  89.2 1.5 reshape.170
  90.7 67.8 %all-gather.14.cloned.1.call-done = bf16[2048,1024]{1,0:T(8,128)(2,1)} async-done(((bf16[256,1024]{1,0:T(8,128)(2,1)}), bf16[2048,1024]{1,0:T(8,128)(2,1)}) %all-gather.14.cloned.1.call-update) | async-done | bytes 4194320 | tf_op jit(solution)/shard_map/all_gather | solution.py:104
  158.5 4.1 convolution_multiply_fusion.5
  162.6 2.4 reshape.171
  165.1 66.9 %all-gather.12.cloned.1.call-done = bf16[2048,1024]{1,0:T(8,128)(2,1)} async-done(((bf16[256,1024]{1,0:T(8,128)(2,1)}), bf16[2048,1024]{1,0:T(8,128)(2,1)}) %all-gather.12.cloned.1.call-update) | async-done | bytes 4194320 | tf_op jit(solution)/shard_map/all_gather | solution.py:106
  232.0 4.0 fusion.55
  236.0 1.3 convert_element_type.112
  237.3 1.3 fusion.70
  238.6 0.2 subtract_convert_fusion
  238.8 0.1 maximum_bitcast_fusion.1
  238.9 0.1 maximum_bitcast_fusion
  238.9 8.3 %while.15 = (s32[]{:T(128)}, f32[4,256,256]{2,1,0:T(8,128)S(1)}, f32[3,4,64,256]{3,2,1,0:T(8,128)}, f32[4]{0:T(128)S(1)}, bf16[3,4,64,256]{3,2,0,1:T(8,128)(2,1)...) while((s32[]{:T(128)}, f32[4,256,256]{2,1,0:T(8,128)S(1)}, ...), condition=%wide.region_2.3_spmd.clone.clone.clone, body=%wide.region_1.2_spmd.clone.clone.clone.sunk | while | flops 420872704 | bytes 4770468 | solution.py:74
  238.9 0.1 multiply_exponential_fusion.4
  239.0 0.8 fusion.98
  239.8 1.0 fusion.99
  240.8 0.8 convolution_add_fusion.3
  241.7 0.1 multiply_exponential_fusion.4
  241.8 0.8 fusion.98
  242.6 1.0 fusion.99
  243.6 0.8 convolution_add_fusion.3
  244.5 0.1 multiply_exponential_fusion.4
  244.5 0.8 fusion.98
  245.4 1.0 fusion.99
  246.4 0.8 convolution_add_fusion.3
  247.2 1.4 multiply_reduce_fusion
  248.6 0.1 copy.57
  248.8 0.3 mul.353
  249.0 0.1 copy.66
  249.2 0.5 copy.53
  249.7 0.1 copy.65
  249.9 57.2 %all-gather.16.cloned.1.call-done = bf16[1024,2048]{1,0:T(8,128)(2,1)} async-done(((bf16[1024,256]{1,0:T(8,128)(2,1)}), bf16[1024,2048]{1,0:T(8,128)(2,1)}) %all-gather.16.cloned.1.call-update) | async-done | bytes 4194320 | tf_op jit(solution)/shard_map/all_gather | solution.py:125
  307.1 4.2 fusion.49
  311.3 0.0 all-gather.22.cloned.1.call-start
  311.4 1.0 convert_element_type.124
  312.4 0.0 all-gather.18.cloned.1.call-start
  312.5 0.5 copy-done.4
  313.0 1.0 convert_element_type.121
  314.0 0.0 all-gather.20.cloned.1.call-start
  314.0 1.0 convert_element_type.122
  315.1 2.7 reduce-scatter.3.cloned.1.call-done
  317.8 1.2 fusion.56
  319.0 1.2 fusion.58
  320.2 2.5 all_gather.35
  322.8 96.9 %all-gather.22.cloned.1.call-done = bf16[12288,256]{1,0:T(8,128)(2,1)} async-done(((bf16[1536,256]{1,0:T(8,128)(2,1)}), bf16[12288,256]{1,0:T(8,128)(2,1)}) %all-gather.22.cloned.1.call-update) | async-done | bytes 6291472 | tf_op jit(solution)/shard_map/all_gather | solution.py:147
  419.7 8.8 %copy.56 = bf16[1536,8,256]{0,2,1:T(8,128)(2,1)} copy(bf16[1536,8,256]{2,0,1:T(8,128)(2,1)} %bitcast.94) | data formatting | bytes 12582912 | tf_op jit(solution)/shard_map/reshape | solution.py:148
  428.5 90.3 %all-gather.18.cloned.1.call-done = bf16[2048,1536]{1,0:T(8,128)(2,1)} async-done(((bf16[256,1536]{1,0:T(8,128)(2,1)}), bf16[2048,1536]{1,0:T(8,128)(2,1)}) %all-gather.18.cloned.1.call-update) | async-done | bytes 6291472 | tf_op jit(solution)/shard_map/all_gather | solution.py:139
  518.8 4.2 convolution_multiply_fusion.2
  523.0 95.0 %all-gather.20.cloned.1.call-done = bf16[2048,1536]{1,0:T(8,128)(2,1)} async-done(((bf16[256,1536]{1,0:T(8,128)(2,1)}), bf16[2048,1536]{1,0:T(8,128)(2,1)}) %all-gather.20.cloned.1.call-update) | async-done | bytes 6291472 | tf_op jit(solution)/shard_map/all_gather | solution.py:140
  617.9 9.0 %fusion.50 = bf16[192,2048]{1,0:T(8,128)(2,1)} fusion(bf16[1536,2048]{0,1:T(8,128)(2,1)} %bitcast.95, f32[2048]{0:T(1024)S(1)} %copy-done.13, bf16[192,2048]{1,0:T(8,128)(2,1)S(1)} %all_gather.35, bf16[2048,1536]{1,0:T(8,128)(2,1)} %all-gather.20.cloned.1.call-done, f32[192,1536]{1,0:T(8,128)S(1)} %convolution_multiply_fusion.2, f32[1536]{0:T(1024)S(1)} %copy-done.14), kind=kOutput, calls=%fused_computation.51 | convolution fusion | flops 2418769920 | bytes 15349760 | tf_op jit(solution)/shard_map/dot_general | solution.py:152
  627.0 6.5 %reduce-scatter.5.cloned.1.call-done = bf16[96,2048]{1,0:T(8,128)(2,1)} async-done(((bf16[192,2048]{1,0:T(8,128)(2,1)}), bf16[96,2048]{1,0:T(8,128)(2,1)}) %reduce-scatter.5.cloned.1.call-update) | async-done | bytes 393232 | tf_op jit(solution)/shard_map/reduce_scatter | solution.py:151
  633.5 1.9 fusion.63
  (60 shorter events, 0.4 us)
Async XLA Ops:
  6.5 2.3 copy-start.6
  6.5 78.5 %all-gather.10.cloned.1.call-start = ((), (), s32[]{:S(2)}) async-start(), calls=%async_computation.2 | async-start | bytes 4718592 | tf_op jit(solution)/shard_map/all_gather | solution.py:105
  8.7 1.4 copy-start.7
  8.8 149.7 %all-gather.14.cloned.1.call-start = ((), (), s32[]{:S(2)}) async-start(), calls=%async_computation.4 | async-start | bytes 4718592 | tf_op jit(solution)/shard_map/all_gather | solution.py:104
  9.7 1.4 copy-start.8
  9.7 222.3 %all-gather.12.cloned.1.call-start = ((), (), s32[]{:S(2)}) async-start(), calls=%async_computation.3 | async-start | bytes 4718592 | tf_op jit(solution)/shard_map/all_gather | solution.py:106
  11.0 1.1 copy-start
  11.1 296.0 %all-gather.16.cloned.1.call-start = ((), (), s32[]{:S(2)}) async-start(), calls=%async_computation.5 | async-start | bytes 4718592 | tf_op jit(solution)/shard_map/all_gather | solution.py:125
  12.0 2.9 copy-start.18
  12.0 73.0 %copy-start.11 = (f32[2048]{0:T(1024)S(1)}, f32[2048]{0:T(1024)}, u32[]{:S(2)}) copy-start(f32[2048]{0:T(1024)} %param.21) | copy-start | bytes 24580
  12.0 73.0 %copy-start.15 = (f32[1024]{0:T(1024)S(1)}, f32[1024]{0:T(1024)}, u32[]{:S(2)}) copy-start(f32[1024]{0:T(1024)} %param.27) | copy-start | bytes 12292
  12.0 305.8 %reduce-scatter.3.cloned.1.call-start = ((), (), s32[]{:S(2)}) async-start(), calls=%async_computation.6 | async-start | bytes 1179648 | tf_op jit(solution)/shard_map/reduce_scatter | solution.py:127
  89.2 69.3 %copy-start.16 = (f32[1024]{0:T(1024)S(1)}, f32[1024]{0:T(1024)}, u32[]{:S(2)}) copy-start(f32[1024]{0:T(1024)} %param.26) | copy-start | bytes 12292
  162.6 69.3 %copy-start.17 = (f32[1024]{0:T(1024)S(1)}, f32[1024]{0:T(1024)}, u32[]{:S(2)}) copy-start(f32[1024]{0:T(1024)} %param.28) | copy-start | bytes 12292
  247.2 2.0 copy-start.2
  249.2 57.9 %copy-start.9 = (f32[2048]{0:T(1024)S(1)}, f32[2048]{0:T(1024)}, u32[]{:S(2)}) copy-start(f32[2048]{0:T(1024)} %param.29) | copy-start | bytes 24580
  307.1 4.3 copy-start.3
  311.3 1.7 copy-start.4
  311.3 108.4 %all-gather.22.cloned.1.call-start = ((), (), s32[]{:S(2)}) async-start(), calls=%async_computation.10 | async-start | bytes 7077888 | tf_op jit(solution)/shard_map/all_gather | solution.py:147
  312.4 1.7 copy-start.5
  312.4 206.4 %all-gather.18.cloned.1.call-start = ((), (), s32[]{:S(2)}) async-start(), calls=%async_computation.7 | async-start | bytes 7077888 | tf_op jit(solution)/shard_map/all_gather | solution.py:139
  314.0 5.1 copy-start.10
  314.0 303.9 %all-gather.20.cloned.1.call-start = ((), (), s32[]{:S(2)}) async-start(), calls=%async_computation.8 | async-start | bytes 7077888 | tf_op jit(solution)/shard_map/all_gather | solution.py:140
  315.1 318.4 %reduce-scatter.5.cloned.1.call-start = ((), (), s32[]{:S(2)}) async-start(), calls=%async_computation.9 | async-start | bytes 1179648 | tf_op jit(solution)/shard_map/reduce_scatter | solution.py:151
  419.7 99.1 %copy-start.12 = (f32[1536]{0:T(1024)S(1)}, f32[1536]{0:T(1024)}, u32[]{:S(2)}) copy-start(f32[1536]{0:T(1024)} %param.35) | copy-start | bytes 18436
  428.5 189.5 %copy-start.13 = (f32[2048]{0:T(1024)S(1)}, f32[2048]{0:T(1024)}, u32[]{:S(2)}) copy-start(f32[2048]{0:T(1024)} %param.37) | copy-start | bytes 24580
  428.5 189.5 %copy-start.14 = (f32[1536]{0:T(1024)S(1)}, f32[1536]{0:T(1024)}, u32[]{:S(2)}) copy-start(f32[1536]{0:T(1024)} %param.36) | copy-start | bytes 18436
  617.9 15.6 %copy-start.1 = (bf16[96,2048]{1,0:T(8,128)(2,1)S(1)}, bf16[96,2048]{1,0:T(8,128)(2,1)}, u32[]{:S(2)}) copy-start(bf16[96,2048]{1,0:T(8,128)(2,1)} %reduce-scatter.3.cloned.1.call-done) | copy-start | bytes 1179652
Sparse Core Ops, SparseCore 0:
  9.5 75.5 all-gather.9
  87.1 71.3 all-gather.13
  160.6 71.3 all-gather.11
  233.9 73.1 all-gather.15
  311.4 6.3 reduce-scatter.2
  319.8 99.8 all-gather.21
  421.9 96.8 all-gather.17
  521.0 96.9 all-gather.19
  627.1 6.3 reduce-scatter.4
